TPU v7x, 32 devices: a whole 2x2x4 slice. The times are simulated.
32 devices in a mesh: sp: 8 (over z, y), tp: 4 (over x, core).
Axes of the slice: x: 2, y: 2, z: 4, core: 2. Of those that a mesh axis runs over, the one named last changes fastest.
Arguments:
- conv_value: bfloat16 [4096, 2048], P('sp', 'tp'), may hold values from -6 to 6
- conv_gate: bfloat16 [4096, 2048], P('sp', 'tp'), may hold values from -6 to 6
- conv_taps: float32 [31, 2048], P(None, 'tp'), as said below
- channel_gain: float32 [2048], P('tp'), may hold values from 0.1 to 1.9
- point_weight: bfloat16 [2048, 2048], replicated, may hold values from -0.125 to 0.125
- residual_in: bfloat16 [4096, 2048], P(('sp', 'tp')), may hold values from -3 to 3
- first_gain: float32 [2048], replicated, may hold values from 0.1 to 1.9
- second_gain: float32 [2048], replicated, may hold values from 0.1 to 1.9
- routes: int32 [4096, 2], P(('sp', 'tp')), may hold values from 0 to 31, all different within a row; in each aligned block of 128 rows (0 to 127, 128 to 255, ...) at most 16 rows name the same one
- route_score: float32 [4096, 2], P(('sp', 'tp')), may hold values from 0.1 to 1
- expert_gate: bfloat16 [32, 2048, 1024], P(('sp', 'tp')), may hold values from -0.125 to 0.125
- expert_up: bfloat16 [32, 2048, 1024], P(('sp', 'tp')), may hold values from -0.125 to 0.125
- expert_down: bfloat16 [32, 1024, 2048], P(('sp', 'tp')), may hold values from -0.1875 to 0.1875
Outputs:
- layer_out: bfloat16 [4096, 2048], P(('sp', 'tp'))
Inputs may be any that keep to these rules, and one draw needn't show every extreme that they name: `routes`: among the 128 rows of one device (aligned blocks of rows), no expert is named more than 16 times, a bound that some block reaches; a row names 2 different experts. conv_taps have independent entries, with scales that differ from channel to channel.
All inputs are finite; a program needn't handle non-finite values.
Results may differ from a plain program's by a relative error of at most 0.013.
Values may be sent and summed in bfloat16 or wider, within the bound.
A program may use at most 128 MiB of HBM per device.

v0:
```python
import functools

import jax
import jax.numpy as jnp
from jax import lax
from jax.experimental import pallas as pl
from jax.experimental.pallas import tpu as pltpu
from jax.sharding import PartitionSpec as P

residual_scale = 8.0**0.25
MESH = pl.DeviceIdType.MESH
VMEM = pl.BlockSpec(memory_space=pltpu.VMEM)


class Grid:
    def __init__(self, sp, tp):
        self.sp, self.tp = sp, tp
        self.planes = 4 if sp % 4 == 0 else 1
        self.inner = sp // self.planes
        self.peers = self.inner * tp

    def here(self):
        s, t = lax.axis_index("sp"), lax.axis_index("tp")
        return s // self.inner, (s % self.inner) * self.tp + t

    def device(self, plane, peer):
        return (plane * self.inner + peer // self.tp, peer % self.tp)

    def greet(self, plane, peer):
        barrier = pltpu.get_barrier_semaphore()
        for d in range(1, self.planes):
            other = self.device((plane + d) % self.planes, peer)
            pl.semaphore_signal(barrier, inc=1, device_id=other, device_id_type=MESH)
        for d in range(1, self.peers):
            other = self.device(plane, (peer + d) % self.peers)
            pl.semaphore_signal(barrier, inc=1, device_id=other, device_id_type=MESH)
        pl.semaphore_wait(barrier, self.planes - 1 + self.peers - 1)


def remote(src, dst, send, recv, device):
    return pltpu.make_async_remote_copy(
        src_ref=src, dst_ref=dst, send_sem=send, recv_sem=recv, device_id=device, device_id_type=MESH
    )


def experts_kernel(
    g, cap, first, table, gain, w_gate, w_up, w_down, final, v_gate, v_up, v_down, hidden, out, tables, held, stage,
    back, sums, came, h2, blk_send, blk_recv, tab_send, tab_recv, row_send, row_recv, own_sem, ans_send, ans_recv,
    ans_own, sum_send, sum_recv, w_sem,
):
    plane, peer = g.here()
    last = g.planes - 1
    slots = g.peers * cap
    above = g.device((plane + 1) % g.planes, peer)
    below = g.device((plane + last) % g.planes, peer)
    loads = [
        pltpu.make_async_copy(src.at[0], dst, w_sem.at[n])
        for n, (src, dst) in enumerate(((w_gate, v_gate), (w_up, v_up), (w_down, v_down)))
    ]
    for load in loads:
        load.start()
    held[plane] = first[...]
    tables[plane] = table[...]
    g.greet(plane, peer)

    def block_copies(src_block, src_table, b, way):
        to = above if way == 0 else below
        return (
            remote(src_block, held.at[b], blk_send.at[way, b], blk_recv.at[b], to),
            remote(src_table, tables.at[b], tab_send.at[way, b], tab_recv.at[b], to),
        )

    def has_way(way):
        return plane < last if way == 0 else plane > 0

    def forward(b, way, own):
        @pl.when(has_way(way))
        def _():
            src = (first, table) if own else (held.at[b], tables.at[b])
            for copy in block_copies(*src, b, way):
                copy.start()

    def place(b):
        number = lax.broadcasted_iota(jnp.int32, (slots, first.shape[0]), 0) + plane * slots
        number = number.astype(jnp.float32)
        rows = tables[b]
        pick = jnp.where((number == rows[0:1]) | (number == rows[1:2]), 1.0, 0.0).astype(jnp.bfloat16)
        stage[b] = jnp.dot(pick, held[b], preferred_element_type=jnp.float32).astype(jnp.bfloat16)
        for d in range(1, g.peers):
            row_copy(b, d).start()
        own_copy(b).start()

    def row_copy(b, d):
        to = (peer + d) % g.peers
        return remote(
            stage.at[b, pl.ds(to * cap, cap)],
            out.at[b, pl.ds(peer * cap, cap)],
            row_send.at[b, d],
            row_recv.at[b, d],
            g.device(plane, to),
        )

    def own_copy(b):
        return pltpu.make_async_copy(
            stage.at[b, pl.ds(peer * cap, cap)], out.at[b, pl.ds(peer * cap, cap)], own_sem.at[b]
        )

    def ans_copy(b, d):
        to = (peer + d) % g.peers
        return remote(
            out.at[b, pl.ds(to * cap, cap)],
            back.at[b, pl.ds(peer * cap, cap)],
            ans_send.at[b, d],
            ans_recv.at[b, d],
            g.device(plane, to),
        )

    def ans_own_copy(b):
        return pltpu.make_async_copy(
            out.at[b, pl.ds(peer * cap, cap)], back.at[b, pl.ds(peer * cap, cap)], ans_own.at[b]
        )

    def spread(b):
        for d in range(1, g.peers):
            ans_copy(b, d).start()
        ans_own_copy(b).start()

    def partial(b):
        ans_own_copy(b).wait()
        for d in range(1, g.peers):
            ans_copy(b, d).wait_recv()
        number = lax.broadcasted_iota(jnp.int32, (slots, first.shape[0]), 0) + plane * slots
        number = number.astype(jnp.float32)
        rows = tables[b]
        weight = jnp.where(number == rows[0:1], rows[2:3], 0.0) + jnp.where(number == rows[1:2], rows[3:4], 0.0)
        weight = weight.T
        high = weight.astype(jnp.bfloat16)
        low = (weight - high.astype(jnp.float32)).astype(jnp.bfloat16)
        got = back[b]
        return jnp.dot(high, got, preferred_element_type=jnp.float32) + jnp.dot(
            low, got, preferred_element_type=jnp.float32
        )

    def sum_copy(b, way):
        return remote(
            sums.at[b], came.at[way, b], sum_send.at[b], sum_recv.at[way, b], above if way == 0 else below
        )

    def steps():
        for s in range(last):
            down = s - (last - plane)
            up = last - s + plane
            yield 1, down, (down >= 0) & (down < plane), plane < last
            yield 0, up, (up > plane) & (up <= last), plane > 0

    cut = 256

    def expert(b):
        own_copy(b).wait()
        for d in range(1, g.peers):
            row_copy(b, d).wait_recv()

        def inner(n, carry):
            at = pl.ds(pl.multiple_of(n * cut, cut), cut)
            rows = out[b]
            gate = jnp.dot(rows, v_gate[:, at], preferred_element_type=jnp.float32)
            upper = jnp.dot(rows, v_up[:, at], preferred_element_type=jnp.float32)
            hidden[:, at] = (gate * jax.nn.sigmoid(gate) * upper).astype(jnp.bfloat16)
            return carry

        lax.fori_loop(0, v_gate.shape[1] // cut, inner, 0)

        def outer(n, carry):
            at = pl.ds(pl.multiple_of(n * cut, cut), cut)
            answer = jnp.dot(hidden[...], v_down[:, at], preferred_element_type=jnp.float32)
            out[b, :, at] = answer.astype(jnp.bfloat16)
            return carry

        lax.fori_loop(0, v_down.shape[1] // cut, outer, 0)
        spread(b)

    for way in range(2):
        forward(plane, way, True)
    place(plane)
    for s in range(1, g.planes + 1):
        for way, b in ((0, plane - s), (1, plane + s)):

            @pl.when((b >= 0) & (b <= last))
            def _():
                for copy in block_copies(held.at[b], tables.at[b], b, way):
                    copy.wait_recv()
                forward(b, way, False)
                place(b)

        if s == 1:
            for load in loads:
                load.wait()
            expert(plane)
        else:
            for b in (plane - s + 1, plane + s - 1):

                @pl.when((b >= 0) & (b <= last))
                def _():
                    expert(b)

    for way, b, valid, relayed in steps():

        @pl.when(valid & relayed)
        def _():
            total = partial(b)
            sum_copy(b, way).wait_recv()
            sums[b] = (total + came[way, b].astype(jnp.float32)).astype(jnp.bfloat16)
            sum_copy(b, way).start()

        @pl.when(valid & jnp.logical_not(relayed))
        def _():
            sums[b] = partial(b).astype(jnp.bfloat16)
            sum_copy(b, way).start()

    h2[...] = residual_scale * first[...].astype(jnp.float32) + partial(plane)
    for way in range(2):

        @pl.when(plane > 0 if way == 0 else plane < last)
        def _():
            sum_copy(plane, way).wait_recv()
            h2[...] += came[way, plane].astype(jnp.float32)

    final[...] = token_norm(h2[...], gain[...]).astype(jnp.bfloat16)
    for way, b, valid, relayed in steps():

        @pl.when(valid)
        def _():
            sum_copy(b, way).wait_send()

    for b in range(g.planes):
        for d in range(1, g.peers):
            ans_copy(b, d).wait_send()

    for s in range(1, g.planes):
        for way, b in ((0, plane - s), (1, plane + s)):

            @pl.when((b >= 0) & (b <= last) & has_way(way))
            def _():
                for copy in block_copies(held.at[b], tables.at[b], b, way):
                    copy.wait_send()

    for way in range(2):

        @pl.when(has_way(way))
        def _():
            for copy in block_copies(first, table, plane, way):
                copy.wait_send()

    for b in range(g.planes):
        for d in range(1, g.peers):
            row_copy(b, d).wait_send()


def experts(g, cap, first, table, gain, w_gate, w_up, w_down):
    rows, width = first.shape
    hidden = w_gate.shape[2]
    slots = g.peers * cap
    dma = pltpu.SemaphoreType.DMA
    f32, bf16 = jnp.float32, jnp.bfloat16
    blocks, pairs = dma((g.planes,)), dma((g.planes, g.peers))
    any_place = pl.BlockSpec(memory_space=pl.ANY)
    return pl.pallas_call(
        functools.partial(experts_kernel, g, cap),
        name="experts",
        out_shape=jax.ShapeDtypeStruct((rows, width), bf16),
        in_specs=[VMEM] * 3 + [any_place] * 3,
        out_specs=VMEM,
        scratch_shapes=[
            pltpu.VMEM((width, hidden), bf16),
            pltpu.VMEM((width, hidden), bf16),
            pltpu.VMEM((hidden, width), bf16),
            pltpu.VMEM((slots, hidden), bf16),
            pltpu.VMEM((g.planes, slots, width), bf16),
            pltpu.VMEM((g.planes,) + table.shape, f32),
            pltpu.VMEM((g.planes, rows, width), bf16),
            pltpu.VMEM((g.planes, slots, width), bf16),
            pltpu.VMEM((g.planes, slots, width), bf16),
            pltpu.VMEM((g.planes, rows, width), bf16),
            pltpu.VMEM((2, g.planes, rows, width), bf16),
            pltpu.VMEM((rows, width), f32),
            dma((2, g.planes)),
            blocks,
            dma((2, g.planes)),
            blocks,
            pairs,
            pairs,
            blocks,
            pairs,
            pairs,
            blocks,
            blocks,
            dma((2, g.planes)),
            dma((3,)),
        ],
        compiler_params=pltpu.CompilerParams(collective_id=0, has_side_effects=True),
    )(first, table, gain, w_gate, w_up, w_down)


def front_kernel(
    sp, tp, value, gate, taps, gain, out, rim_v, rim_g, glu, conv, part1, part2, stat, stats, cols, stage,
    rim_send, rim_recv, stat_send, stat_recv, act_send, act_recv, own_sem,
):
    s, t = lax.axis_index("sp"), lax.axis_index("tp")
    tokens, width = value.shape
    kw = taps.shape[0]
    pad = rim_v.shape[0]
    rows = tokens // tp
    lead = pad - (kw - 1)
    tile = 64
    lane = 128

    barrier = pltpu.get_barrier_semaphore()
    for other in ((s + 1) % sp, (s + sp - 1) % sp):
        pl.semaphore_signal(barrier, inc=1, device_id=(other, t), device_id_type=MESH)
    for d in range(1, tp):
        pl.semaphore_signal(barrier, inc=1, device_id=(s, (t + d) % tp), device_id_type=MESH)
    pl.semaphore_wait(barrier, 2 + tp - 1)

    def rims():
        to = ((s + 1) % sp, t)
        tail = pl.ds(tokens - pad, pad)
        return (
            remote(value.at[tail], rim_v, rim_send.at[0], rim_recv.at[0], to),
            remote(gate.at[tail], rim_g, rim_send.at[1], rim_recv.at[1], to),
        )

    @pl.when(s < sp - 1)
    def _():
        for copy in rims():
            copy.start()

    def gated(v, g):
        return v.astype(jnp.float32) * jax.nn.sigmoid(g.astype(jnp.float32))

    def glu_tile(i, carry):
        at = pl.multiple_of(i * tile, tile)
        glu[pl.ds(pad + at, tile)] = gated(value[pl.ds(at, tile)], gate[pl.ds(at, tile)])
        return carry

    lax.fori_loop(0, tokens // tile, glu_tile, 0)

    def conv_tile(i, carry):
        at = pl.multiple_of(i * tile, tile)
        one = two = None
        for c in range(width // lane):
            lanes = pl.ds(c * lane, lane)
            total = None
            for r in range(8):
                piece = None
                extra = 8 if r else 0
                for m in range(pad // 8 + 1):
                    j = 8 * m + r - lead
                    if 0 <= j < kw:
                        term = taps[j : j + 1, lanes] * glu[pl.ds(at + 8 * m, tile + extra), lanes]
                        piece = term if piece is None else piece + term
                if piece is not None:
                    piece = piece[r : r + tile]
                    total = piece if total is None else total + piece
            conv[pl.ds(at, tile), lanes] = total
            one = total if one is None else one + total
            two = total * total if two is None else two + total * total
        part1[pl.ds(at, tile)] = one
        part2[pl.ds(at, tile)] = two
        return carry

    lax.fori_loop(1, tokens // tile, conv_tile, 0)

    @pl.when(s > 0)
    def _():
        for copy in rims():
            copy.wait_recv()
        glu[pl.ds(0, pad)] = gated(rim_v[...], rim_g[...])

    @pl.when(s == 0)
    def _():
        glu[pl.ds(0, pad)] = jnp.zeros((pad, width), jnp.float32)

    conv_tile(0, 0)

    ones = jnp.ones((8, lane), jnp.float32)

    def row_sums(part):
        return lax.dot_general(
            ones,
            part[...],
            (((1,), (1,)), ((), ())),
            precision=lax.Precision.HIGHEST,
            preferred_element_type=jnp.float32,
        )

    first_row = lax.broadcasted_iota(jnp.int32, (8, tokens), 0) == 0
    mine = jnp.where(first_row, row_sums(part1), row_sums(part2))
    stat[...] = mine

    def stat_copy(d):
        return remote(stat, stats.at[d], stat_send.at[d], stat_recv.at[d], (s, (t + d) % tp))

    for d in range(1, tp):
        stat_copy(d).start()
    for d in range(1, tp):
        stat_copy(d).wait_recv()
        mine = mine + stats[d]
    scaled = mine / (width * tp)
    middle = scaled[0:1]
    factor = lax.rsqrt(scaled[1:2] - middle * middle + 1e-05)
    cols[...] = jnp.where(first_row, middle, factor).T

    def act_copy(d):
        to = (t + d) % tp
        return remote(
            stage.at[d],
            out.at[:, pl.ds(pl.multiple_of(t * width, width), width)],
            act_send.at[d],
            act_recv.at[d],
            (s, to),
        )

    own = pltpu.make_async_copy(stage.at[0], out.at[:, pl.ds(pl.multiple_of(t * width, width), width)], own_sem)
    for d in list(range(1, tp)) + [0]:
        at = pl.multiple_of((t + d) % tp * rows, rows)
        side = cols[pl.ds(at, rows)]
        normed = (conv[pl.ds(at, rows)] - side[:, 0:1]) * side[:, 1:2] * gain[...]
        stage[d] = (normed * jax.nn.sigmoid(normed)).astype(jnp.bfloat16)
        if d:
            act_copy(d).start()
        else:
            own.start()
    own.wait()
    for d in range(1, tp):
        act_copy(d).wait()
        stat_copy(d).wait_send()

    @pl.when(s < sp - 1)
    def _():
        for copy in rims():
            copy.wait_send()


def front(sp, tp, value, gate, taps, gain):
    tokens, width = value.shape
    pad = -(-(taps.shape[0] - 1) // 16) * 16
    rows = tokens // tp
    dma = pltpu.SemaphoreType.DMA
    f32, bf16 = jnp.float32, jnp.bfloat16
    return pl.pallas_call(
        functools.partial(front_kernel, sp, tp),
        name="front",
        out_shape=jax.ShapeDtypeStruct((rows, width * tp), bf16),
        in_specs=[VMEM] * 4,
        out_specs=VMEM,
        scratch_shapes=[
            pltpu.VMEM((pad, width), bf16),
            pltpu.VMEM((pad, width), bf16),
            pltpu.VMEM((pad + tokens, width), f32),
            pltpu.VMEM((tokens, width), f32),
            pltpu.VMEM((tokens, 128), f32),
            pltpu.VMEM((tokens, 128), f32),
            pltpu.VMEM((8, tokens), f32),
            pltpu.VMEM((tp, 8, tokens), f32),
            pltpu.VMEM((tokens, 8), f32),
            pltpu.VMEM((tp, rows, width), bf16),
            dma((2,)),
            dma((2,)),
            dma((tp,)),
            dma((tp,)),
            dma((tp,)),
            dma((tp,)),
            dma,
        ],
        compiler_params=pltpu.CompilerParams(collective_id=2, has_side_effects=True),
    )(value, gate, taps, gain)


def token_norm(values, gain):
    middle = jnp.mean(values, axis=-1, keepdims=True)
    centred = values - middle
    spread = jnp.mean(centred * centred, axis=-1, keepdims=True)
    return centred * lax.rsqrt(spread + 1e-05) * gain


def per_device(
    conv_value,
    conv_gate,
    conv_taps,
    channel_gain,
    point_weight,
    residual_in,
    first_gain,
    second_gain,
    routes,
    route_score,
    expert_gate,
    expert_up,
    expert_down,
):
    owned = front(
        lax.axis_size("sp"), lax.axis_size("tp"), conv_value, conv_gate, conv_taps, channel_gain[None]
    )
    rows = owned.shape[0]
    mix = jnp.dot(owned, point_weight, preferred_element_type=jnp.float32)
    first = token_norm(residual_scale * residual_in.astype(jnp.float32) + mix, first_gain).astype(
        jnp.bfloat16
    )
    top = routes.shape[1]
    g = Grid(lax.axis_size("sp"), lax.axis_size("tp"))
    count = g.planes * g.peers
    most = max(2, 2 * rows * top // count)
    cap = -(-most // 16) * 16
    flat_e = routes.reshape(-1)
    onehot = (flat_e[:, None] == jnp.arange(count, dtype=jnp.int32)[None, :]).astype(jnp.int32)
    before = jnp.sum((jnp.cumsum(onehot, axis=0) - onehot) * onehot, axis=1)
    slot = (flat_e * cap + before).reshape(rows, top).astype(jnp.float32)
    share = route_score / jnp.sum(route_score, axis=1, keepdims=True)
    table = jnp.concatenate([slot, share, jnp.zeros((rows, 4), jnp.float32)], axis=1).T
    return experts(g, cap, first, table, second_gain[None], expert_gate, expert_up, expert_down)


def solution(mesh):
    in_specs = (
        P("sp", "tp"),
        P("sp", "tp"),
        P(None, "tp"),
        P("tp"),
        P(),
        P(("sp", "tp"), None),
        P(),
        P(),
        P(("sp", "tp"), None),
        P(("sp", "tp"), None),
        P(("sp", "tp"), None, None),
        P(("sp", "tp"), None, None),
        P(("sp", "tp"), None, None),
    )
    out_specs = P(("sp", "tp"), None)
    return jax.shard_map(
        per_device, mesh=mesh, in_specs=in_specs, out_specs=out_specs, check_vma=False
    )
```

profile of v0, /device:TPU:0, one launch (start us, length us, event | category | flops | bytes accessed | tf_op | source)
XLA Modules:
  0.0 135.0 jit_solution(4756921026034107104)
XLA Ops:
  0.0 21.7 %front.1 = bf16[128,2048]{1,0:T(8,128)(2,1)} custom-call(bf16[512,512]{1,0:T(8,128)(2,1)} %value.1, bf16[512,512]{1,0:T(8,128)(2,1)} %gate.1, f32[31,512]{1,0:T(8,128)} %taps.1, f32[1,512]{1,0:T(1,128)} %bitcast.26), custom_call_target="tpu_custom_call" | custom-call | tf_op jit(solution)/shard_map/front/pallas_call | solution.py:450
  21.7 0.0 copy-start
  21.7 0.0 copy-start.1
  21.7 0.0 copy-start.2
  21.7 5.0 %fusion.4 = (f32[128]{0:T(128)S(1)}, f32[128,2048]{1,0:T(8,128)S(1)}) fusion(bf16[128,2048]{1,0:T(8,128)(2,1)} %front.1, bf16[2048,2048]{1,0:T(8,128)(2,1)} %param.17, bf16[128,2048]{1,0:T(8,128)(2,1)} %param.18), kind=kOutput, calls=%fused_computation.17 | convolution fusion | flops 1074790272 | bytes 10486272 | tf_op jit(solution)/shard_map/dot_general | solution.py:505
  26.7 0.3 multiply_reduce_fusion
  27.0 0.0 copy-done
  27.0 1.0 multiply_convert_fusion.first
  28.0 0.0 copy-done.1
  28.0 0.1 copy.14
  28.1 0.1 eq.29
  28.3 0.6 reduce-window.6
  28.9 0.2 slice_reduce_fusion
  29.1 0.1 eq.25
  29.2 0.1 fusion.2
  29.3 0.1 reduce_sum.41
  29.5 0.1 copy.17
  29.6 0.0 copy-done.2
  29.6 0.1 pad.2.clone
  29.7 0.7 maximum_bitcast_fusion.table
  30.4 102.7 %experts.1 = bf16[128,2048]{1,0:T(8,128)(2,1)} custom-call(bf16[128,2048]{1,0:T(8,128)(2,1)} %multiply_convert_fusion.first, f32[8,128]{1,0:T(8,128)} %maximum_bitcast_fusion.table, f32[1,2048]{1,0:T(1,128)} %bitcast.25, bf16[1,2048,1024]{2,1,0:T(8,128)(2,1)} %w_gate.1, bf16[1,2048,1024]{2,1,0:T(8,128)(2,1)} %w_up.1, bf16[1,1024,2048]{2,1,0:T(8,128)(2,1)} %w_down.1), custom_call_target="tpu_custom_call" | custom-call | tf_op jit(solution)/shard_map/experts/pallas_call | solution.py:267
  133.1 1.9 %copy.21 = bf16[128,2048]{1,0:T(8,128)(2,1)} copy(bf16[128,2048]{1,0:T(8,128)(2,1)} %experts.1) | data formatting | bytes 1048576
  (9 shorter events, 0.1 us)
Async XLA Ops:
  21.7 5.3 %copy-start = (f32[2048]{0:T(1024)S(1)}, f32[2048]{0:T(1024)}, u32[]{:S(2)}) copy-start(f32[2048]{0:T(1024)} %param.19) | copy-start | bytes 24580
  21.7 6.3 %copy-start.1 = (s32[128,2]{0,1:T(2,128)S(1)}, s32[128,2]{0,1:T(2,128)}, u32[]{:S(2)}) copy-start(s32[128,2]{0,1:T(2,128)} %param.21) | copy-start | bytes 3076
  21.7 7.8 %copy-start.2 = (f32[128,2]{0,1:T(2,128)S(1)}, f32[128,2]{0,1:T(2,128)}, u32[]{:S(2)}) copy-start(f32[128,2]{0,1:T(2,128)} %param.22) | copy-start | bytes 3076
where the time goes:
time: 135 us
  Pallas kernels  124 us (92%)
  matrix products  4.97 us (4%)
  local copies, waits for them, and re-layouts  2.76 us (2%)
  other arithmetic  2.72 us (2%)
    pallas_call x1, Pallas kernels, experts(): pl.pallas_call(functools.partial(experts_kernel, g, cap), name='experts',...  103 us
    pallas_call x1, Pallas kernels, front(): pl.pallas_call(functools.partial(front_kernel, sp, tp), name='front', out...  21.7 us
    dot_general x1, matrix products, per_device(): mix = jnp.dot(owned, point_weight, preferred_element_type=jnp.float32)  4.97 us

commit v1 on v0

--- a/solution.py
+++ b/solution.py
@@ -44,13 +44,15 @@
 
 
 def experts_kernel(
-    g, cap, first, table, gain, w_gate, w_up, w_down, final, v_gate, v_up, v_down, hidden, out, tables, held, stage,
-    back, sums, came, h2, blk_send, blk_recv, tab_send, tab_recv, row_send, row_recv, own_sem, ans_send, ans_recv,
-    ans_own, sum_send, sum_recv, w_sem,
+    g, cap, parts, first, table, gain, w_gate, w_up, w_down, final, v_gate, v_up, v_down, hidden, out, tables, held,
+    stage, back, sums, came, h2, share, blk_send, blk_recv, tab_send, tab_recv, row_send, row_recv, own_sem, ans_send,
+    ans_recv, ans_own, sum_send, sum_recv, w_sem,
 ):
     plane, peer = g.here()
     last = g.planes - 1
+    rows, width = first.shape
     slots = g.peers * cap
+    part = width // parts
     above = g.device((plane + 1) % g.planes, peer)
     below = g.device((plane + last) % g.planes, peer)
     loads = [
@@ -63,209 +65,237 @@
     tables[plane] = table[...]
     g.greet(plane, peer)
 
-    def block_copies(src_block, src_table, b, way):
-        to = above if way == 0 else below
-        return (
-            remote(src_block, held.at[b], blk_send.at[way, b], blk_recv.at[b], to),
-            remote(src_table, tables.at[b], tab_send.at[way, b], tab_recv.at[b], to),
+    def cols(c):
+        return pl.ds(c * part, part)
+
+    def mine(at):
+        return pl.ds(pl.multiple_of(at * cap, cap), cap)
+
+    def table_copy(b, way, own):
+        src = table if own else tables.at[b]
+        return remote(src, tables.at[b], tab_send.at[way, b], tab_recv.at[b], above if way == 0 else below)
+
+    def block_copy(b, way, c, own):
+        src = first.at[:, cols(c)] if own else held.at[b, :, cols(c)]
+        return remote(
+            src, held.at[b, :, cols(c)], blk_send.at[way, b, c], blk_recv.at[b, c], above if way == 0 else below
         )
 
     def has_way(way):
         return plane < last if way == 0 else plane > 0
 
-    def forward(b, way, own):
+    def near(s):
+        return [(way, b, (b >= 0) & (b <= last)) for way, b in ((0, plane - s), (1, plane + s))]
+
+    def numbers():
+        number = lax.broadcasted_iota(jnp.int32, (slots, rows), 0) + plane * slots
+        return number.astype(jnp.float32)
+
+    def weigh(b):
+        number = numbers()
+        t = tables[b]
+        weight = jnp.where(number == t[0:1], t[2:3], 0.0) + jnp.where(number == t[1:2], t[3:4], 0.0)
+        weight = weight.T
+        high = weight.astype(jnp.bfloat16)
+        share[b, 0] = high
+        share[b, 1] = (weight - high.astype(jnp.float32)).astype(jnp.bfloat16)
+
+    def place(b, c):
+        number = numbers()
+        t = tables[b]
+        pick = jnp.where((number == t[0:1]) | (number == t[1:2]), 1.0, 0.0).astype(jnp.bfloat16)
+        picked = jnp.dot(pick, held[b, :, cols(c)], preferred_element_type=jnp.float32)
+        stage[b, :, cols(c)] = picked.astype(jnp.bfloat16)
+        for d in range(1, g.peers):
+            row_copy(b, d, c).start()
+        own_copy(b, c).start()
+
+    def row_copy(b, d, c):
+        to = (peer + d) % g.peers
+        return remote(
+            stage.at[b, mine(to), cols(c)],
+            out.at[b, mine(peer), cols(c)],
+            row_send.at[b, d, c],
+            row_recv.at[b, d, c],
+            g.device(plane, to),
+        )
+
+    def own_copy(b, c):
+        return pltpu.make_async_copy(stage.at[b, mine(peer), cols(c)], out.at[b, mine(peer), cols(c)], own_sem.at[b, c])
+
+    def ans_copy(b, d, c):
+        to = (peer + d) % g.peers
+        return remote(
+            out.at[b, mine(to), cols(c)],
+            back.at[b, mine(peer), cols(c)],
+            ans_send.at[b, d, c],
+            ans_recv.at[b, d, c],
+            g.device(plane, to),
+        )
+
+    def ans_own_copy(b, c):
+        return pltpu.make_async_copy(out.at[b, mine(peer), cols(c)], back.at[b, mine(peer), cols(c)], ans_own.at[b, c])
+
+    def partial(b, c):
+        ans_own_copy(b, c).wait()
+        for d in range(1, g.peers):
+            ans_copy(b, d, c).wait_recv()
+        got = back[b, :, cols(c)]
+        return jnp.dot(share[b, 0], got, preferred_element_type=jnp.float32) + jnp.dot(
+            share[b, 1], got, preferred_element_type=jnp.float32
+        )
+
+    def sum_copy(b, way, c):
+        return remote(
+            sums.at[b, :, cols(c)],
+            came.at[way, b, :, cols(c)],
+            sum_send.at[b, c],
+            sum_recv.at[way, b, c],
+            above if way == 0 else below,
+        )
+
+    def chains(k):
+        yield 0, k, k > plane, plane > 0
+        yield 1, last - k, last - k < plane, plane < last
+
+    cut = 256
+
+    def expert(b):
+        for c in range(parts):
+            own_copy(b, c).wait()
+            for d in range(1, g.peers):
+                row_copy(b, d, c).wait_recv()
+
+        def inner(n, carry):
+            at = pl.ds(pl.multiple_of(n * cut, cut), cut)
+            x = out[b]
+            gate = jnp.dot(x, v_gate[:, at], preferred_element_type=jnp.float32)
+            upper = jnp.dot(x, v_up[:, at], preferred_element_type=jnp.float32)
+            hidden[:, at] = (gate * jax.nn.sigmoid(gate) * upper).astype(jnp.bfloat16)
+            return carry
+
+        lax.fori_loop(0, v_gate.shape[1] // cut, inner, 0)
+        for c in range(parts):
+            answer = jnp.dot(hidden[...], v_down[:, cols(c)], preferred_element_type=jnp.float32)
+            out[b, :, cols(c)] = answer.astype(jnp.bfloat16)
+            for d in range(1, g.peers):
+                ans_copy(b, d, c).start()
+            ans_own_copy(b, c).start()
+
+    def experts_near(s):
+        for way, b, valid in near(s):
+            pl.when(valid)(functools.partial(expert, b))
+
+    def combine(k, c):
+        for way, b, valid, relayed in chains(k):
+
+            @pl.when(valid & relayed)
+            def _():
+                total = partial(b, c)
+                sum_copy(b, way, c).wait_recv()
+                sums[b, :, cols(c)] = (total + came[way, b, :, cols(c)].astype(jnp.float32)).astype(jnp.bfloat16)
+                sum_copy(b, way, c).start()
+
+            @pl.when(valid & jnp.logical_not(relayed))
+            def _():
+                sums[b, :, cols(c)] = partial(b, c).astype(jnp.bfloat16)
+                sum_copy(b, way, c).start()
+
+    def arrive(s, c):
+        for way, b, valid in near(s):
+
+            @pl.when(valid)
+            def _():
+                if c == 0:
+                    table_copy(b, way, False).wait_recv()
+
+                    @pl.when(has_way(way))
+                    def _():
+                        table_copy(b, way, False).start()
+
+                block_copy(b, way, c, False).wait_recv()
+
+                @pl.when(has_way(way))
+                def _():
+                    block_copy(b, way, c, False).start()
+
+                place(b, c)
+                if c == 0:
+                    weigh(b)
+
+    for way in range(2):
+
         @pl.when(has_way(way))
         def _():
-            src = (first, table) if own else (held.at[b], tables.at[b])
-            for copy in block_copies(*src, b, way):
-                copy.start()
-
-    def place(b):
-        number = lax.broadcasted_iota(jnp.int32, (slots, first.shape[0]), 0) + plane * slots
-        number = number.astype(jnp.float32)
-        rows = tables[b]
-        pick = jnp.where((number == rows[0:1]) | (number == rows[1:2]), 1.0, 0.0).astype(jnp.bfloat16)
-        stage[b] = jnp.dot(pick, held[b], preferred_element_type=jnp.float32).astype(jnp.bfloat16)
-        for d in range(1, g.peers):
-            row_copy(b, d).start()
-        own_copy(b).start()
-
-    def row_copy(b, d):
-        to = (peer + d) % g.peers
-        return remote(
-            stage.at[b, pl.ds(to * cap, cap)],
-            out.at[b, pl.ds(peer * cap, cap)],
-            row_send.at[b, d],
-            row_recv.at[b, d],
-            g.device(plane, to),
-        )
-
-    def own_copy(b):
-        return pltpu.make_async_copy(
-            stage.at[b, pl.ds(peer * cap, cap)], out.at[b, pl.ds(peer * cap, cap)], own_sem.at[b]
-        )
-
-    def ans_copy(b, d):
-        to = (peer + d) % g.peers
-        return remote(
-            out.at[b, pl.ds(to * cap, cap)],
-            back.at[b, pl.ds(peer * cap, cap)],
-            ans_send.at[b, d],
-            ans_recv.at[b, d],
-            g.device(plane, to),
-        )
-
-    def ans_own_copy(b):
-        return pltpu.make_async_copy(
-            out.at[b, pl.ds(peer * cap, cap)], back.at[b, pl.ds(peer * cap, cap)], ans_own.at[b]
-        )
-
-    def spread(b):
-        for d in range(1, g.peers):
-            ans_copy(b, d).start()
-        ans_own_copy(b).start()
-
-    def partial(b):
-        ans_own_copy(b).wait()
-        for d in range(1, g.peers):
-            ans_copy(b, d).wait_recv()
-        number = lax.broadcasted_iota(jnp.int32, (slots, first.shape[0]), 0) + plane * slots
-        number = number.astype(jnp.float32)
-        rows = tables[b]
-        weight = jnp.where(number == rows[0:1], rows[2:3], 0.0) + jnp.where(number == rows[1:2], rows[3:4], 0.0)
-        weight = weight.T
-        high = weight.astype(jnp.bfloat16)
-        low = (weight - high.astype(jnp.float32)).astype(jnp.bfloat16)
-        got = back[b]
-        return jnp.dot(high, got, preferred_element_type=jnp.float32) + jnp.dot(
-            low, got, preferred_element_type=jnp.float32
-        )
-
-    def sum_copy(b, way):
-        return remote(
-            sums.at[b], came.at[way, b], sum_send.at[b], sum_recv.at[way, b], above if way == 0 else below
-        )
-
-    def steps():
-        for s in range(last):
-            down = s - (last - plane)
-            up = last - s + plane
-            yield 1, down, (down >= 0) & (down < plane), plane < last
-            yield 0, up, (up > plane) & (up <= last), plane > 0
-
-    cut = 256
-
-    def expert(b):
-        own_copy(b).wait()
-        for d in range(1, g.peers):
-            row_copy(b, d).wait_recv()
-
-        def inner(n, carry):
-            at = pl.ds(pl.multiple_of(n * cut, cut), cut)
-            rows = out[b]
-            gate = jnp.dot(rows, v_gate[:, at], preferred_element_type=jnp.float32)
-            upper = jnp.dot(rows, v_up[:, at], preferred_element_type=jnp.float32)
-            hidden[:, at] = (gate * jax.nn.sigmoid(gate) * upper).astype(jnp.bfloat16)
-            return carry
-
-        lax.fori_loop(0, v_gate.shape[1] // cut, inner, 0)
-
-        def outer(n, carry):
-            at = pl.ds(pl.multiple_of(n * cut, cut), cut)
-            answer = jnp.dot(hidden[...], v_down[:, at], preferred_element_type=jnp.float32)
-            out[b, :, at] = answer.astype(jnp.bfloat16)
-            return carry
-
-        lax.fori_loop(0, v_down.shape[1] // cut, outer, 0)
-        spread(b)
-
+            table_copy(plane, way, True).start()
+            for c in range(parts):
+                block_copy(plane, way, c, True).start()
+
+    for c in range(parts):
+        place(plane, c)
+    weigh(plane)
+    for s in range(1, g.planes + 1):
+        for c in range(parts):
+            if s < g.planes:
+                arrive(s, c)
+            if s == 1 and c == parts - 2:
+                for load in loads:
+                    load.wait()
+                expert(plane)
+            if s > 1 and c == 0:
+                experts_near(s - 1)
+            if s == 2 and c == parts - 2:
+                for n in range(parts):
+                    h2[:, cols(n)] = residual_scale * first[:, cols(n)].astype(jnp.float32) + partial(plane, n)
+            if s == g.planes:
+                combine(s - 1, c)
+            elif s > 1 and c == parts - 2:
+                for n in range(parts // 2):
+                    combine(s - 1, n)
+            elif s > 1 and c == parts - 1:
+                for n in range(parts // 2, parts):
+                    combine(s - 1, n)
+
+    for c in range(parts):
+        for way in range(2):
+
+            @pl.when(plane > 0 if way == 0 else plane < last)
+            def _():
+                sum_copy(plane, way, c).wait_recv()
+                h2[:, cols(c)] += came[way, plane, :, cols(c)].astype(jnp.float32)
+
+    final[...] = token_norm(h2[...], gain[...]).astype(jnp.bfloat16)
+    for c in range(parts):
+        for k in range(1, g.planes):
+            for way, b, valid, relayed in chains(k):
+                pl.when(valid)(lambda: sum_copy(b, way, c).wait_send())
+        for b in range(g.planes):
+            for d in range(1, g.peers):
+                ans_copy(b, d, c).wait_send()
+                row_copy(b, d, c).wait_send()
+        for s in range(1, g.planes):
+            for way, b, valid in near(s):
+                pl.when(valid & has_way(way))(lambda: block_copy(b, way, c, False).wait_send())
+        for way in range(2):
+            pl.when(has_way(way))(lambda: block_copy(plane, way, c, True).wait_send())
+    for s in range(1, g.planes):
+        for way, b, valid in near(s):
+            pl.when(valid & has_way(way))(lambda: table_copy(b, way, False).wait_send())
     for way in range(2):
-        forward(plane, way, True)
-    place(plane)
-    for s in range(1, g.planes + 1):
-        for way, b in ((0, plane - s), (1, plane + s)):
-
-            @pl.when((b >= 0) & (b <= last))
-            def _():
-                for copy in block_copies(held.at[b], tables.at[b], b, way):
-                    copy.wait_recv()
-                forward(b, way, False)
-                place(b)
-
-        if s == 1:
-            for load in loads:
-                load.wait()
-            expert(plane)
-        else:
-            for b in (plane - s + 1, plane + s - 1):
-
-                @pl.when((b >= 0) & (b <= last))
-                def _():
-                    expert(b)
-
-    for way, b, valid, relayed in steps():
-
-        @pl.when(valid & relayed)
-        def _():
-            total = partial(b)
-            sum_copy(b, way).wait_recv()
-            sums[b] = (total + came[way, b].astype(jnp.float32)).astype(jnp.bfloat16)
-            sum_copy(b, way).start()
-
-        @pl.when(valid & jnp.logical_not(relayed))
-        def _():
-            sums[b] = partial(b).astype(jnp.bfloat16)
-            sum_copy(b, way).start()
-
-    h2[...] = residual_scale * first[...].astype(jnp.float32) + partial(plane)
-    for way in range(2):
-
-        @pl.when(plane > 0 if way == 0 else plane < last)
-        def _():
-            sum_copy(plane, way).wait_recv()
-            h2[...] += came[way, plane].astype(jnp.float32)
-
-    final[...] = token_norm(h2[...], gain[...]).astype(jnp.bfloat16)
-    for way, b, valid, relayed in steps():
-
-        @pl.when(valid)
-        def _():
-            sum_copy(b, way).wait_send()
-
-    for b in range(g.planes):
-        for d in range(1, g.peers):
-            ans_copy(b, d).wait_send()
-
-    for s in range(1, g.planes):
-        for way, b in ((0, plane - s), (1, plane + s)):
-
-            @pl.when((b >= 0) & (b <= last) & has_way(way))
-            def _():
-                for copy in block_copies(held.at[b], tables.at[b], b, way):
-                    copy.wait_send()
-
-    for way in range(2):
-
-        @pl.when(has_way(way))
-        def _():
-            for copy in block_copies(first, table, plane, way):
-                copy.wait_send()
-
-    for b in range(g.planes):
-        for d in range(1, g.peers):
-            row_copy(b, d).wait_send()
+        pl.when(has_way(way))(lambda: table_copy(plane, way, True).wait_send())
 
 
 def experts(g, cap, first, table, gain, w_gate, w_up, w_down):
     rows, width = first.shape
     hidden = w_gate.shape[2]
     slots = g.peers * cap
+    parts = 4
     dma = pltpu.SemaphoreType.DMA
     f32, bf16 = jnp.float32, jnp.bfloat16
-    blocks, pairs = dma((g.planes,)), dma((g.planes, g.peers))
+    blocks, pairs = dma((g.planes, parts)), dma((g.planes, g.peers, parts))
     any_place = pl.BlockSpec(memory_space=pl.ANY)
     return pl.pallas_call(
-        functools.partial(experts_kernel, g, cap),
+        functools.partial(experts_kernel, g, cap, parts),
         name="experts",
         out_shape=jax.ShapeDtypeStruct((rows, width), bf16),
         in_specs=[VMEM] * 3 + [any_place] * 3,
@@ -283,10 +313,11 @@
             pltpu.VMEM((g.planes, rows, width), bf16),
             pltpu.VMEM((2, g.planes, rows, width), bf16),
             pltpu.VMEM((rows, width), f32),
-            dma((2, g.planes)),
+            pltpu.VMEM((g.planes, 2, rows, slots), bf16),
+            dma((2, g.planes, parts)),
             blocks,
             dma((2, g.planes)),
-            blocks,
+            dma((g.planes,)),
             pairs,
             pairs,
             blocks,
@@ -294,7 +325,7 @@
             pairs,
             blocks,
             blocks,
-            dma((2, g.planes)),
+            dma((2, g.planes, parts)),
             dma((3,)),
         ],
         compiler_params=pltpu.CompilerParams(collective_id=0, has_side_effects=True),

time: 135 us -> 144 us (1.067)
  Pallas kernels: 124 us -> 133 us
    pallas_call x1, Pallas kernels: 103 us -> 111 us  [experts(): pl.pallas_call(functools.partial(experts_kernel, g, cap, parts), name='ex...]
where the time goes in v1:
time: 144 us; the launch traced here: 143 us
  Pallas kernels  133 us (92%)
  matrix products  4.97 us (3%)
  local copies, waits for them, and re-layouts  2.76 us (2%)
  other arithmetic  2.72 us (2%)
    pallas_call x1, Pallas kernels, experts(): pl.pallas_call(functools.partial(experts_kernel, g, cap, parts), name='ex...  111 us
    pallas_call x1, Pallas kernels, front(): pl.pallas_call(functools.partial(front_kernel, sp, tp), name='front', out...  21.7 us
    dot_general x1, matrix products, per_device(): mix = jnp.dot(owned, point_weight, preferred_element_type=jnp.float32)  4.97 us

profile of v1, /device:TPU:0, one launch (start us, length us, event | category | flops | bytes accessed | tf_op | source)
XLA Modules:
  0.0 143.3 jit_solution(6538763121437063532)
XLA Ops:
  0.0 21.7 %front.1 = bf16[128,2048]{1,0:T(8,128)(2,1)} custom-call(bf16[512,512]{1,0:T(8,128)(2,1)} %value.1, bf16[512,512]{1,0:T(8,128)(2,1)} %gate.1, f32[31,512]{1,0:T(8,128)} %taps.1, f32[1,512]{1,0:T(1,128)} %bitcast.26), custom_call_target="tpu_custom_call" | custom-call | tf_op jit(solution)/shard_map/front/pallas_call | solution.py:481
  21.7 0.0 copy-start
  21.7 0.0 copy-start.1
  21.7 0.0 copy-start.2
  21.7 5.0 %fusion.4 = (f32[128]{0:T(128)S(1)}, f32[128,2048]{1,0:T(8,128)S(1)}) fusion(bf16[128,2048]{1,0:T(8,128)(2,1)} %front.1, bf16[2048,2048]{1,0:T(8,128)(2,1)} %param.17, bf16[128,2048]{1,0:T(8,128)(2,1)} %param.18), kind=kOutput, calls=%fused_computation.17 | convolution fusion | flops 1074790272 | bytes 10486272 | tf_op jit(solution)/shard_map/dot_general | solution.py:536
  26.7 0.3 multiply_reduce_fusion
  27.0 0.0 copy-done
  27.0 1.0 multiply_convert_fusion.first
  28.0 0.0 copy-done.1
  28.0 0.1 copy.14
  28.1 0.1 eq.29
  28.3 0.6 reduce-window.6
  28.9 0.2 slice_reduce_fusion
  29.1 0.1 eq.25
  29.2 0.1 fusion.2
  29.3 0.1 reduce_sum.41
  29.5 0.1 copy.17
  29.6 0.0 copy-done.2
  29.6 0.1 pad.2.clone
  29.7 0.7 maximum_bitcast_fusion.table
  30.4 111.1 %experts.1 = bf16[128,2048]{1,0:T(8,128)(2,1)} custom-call(bf16[128,2048]{1,0:T(8,128)(2,1)} %multiply_convert_fusion.first, f32[8,128]{1,0:T(8,128)} %maximum_bitcast_fusion.table, f32[1,2048]{1,0:T(1,128)} %bitcast.25, bf16[1,2048,1024]{2,1,0:T(8,128)(2,1)} %w_gate.1, bf16[1,2048,1024]{2,1,0:T(8,128)(2,1)} %w_up.1, bf16[1,1024,2048]{2,1,0:T(8,128)(2,1)} %w_down.1), custom_call_target="tpu_custom_call" | custom-call | tf_op jit(solution)/shard_map/experts/pallas_call | solution.py:297
  141.5 1.9 %copy.21 = bf16[128,2048]{1,0:T(8,128)(2,1)} copy(bf16[128,2048]{1,0:T(8,128)(2,1)} %experts.1) | data formatting | bytes 1048576
  (9 shorter events, 0.1 us)
Async XLA Ops:
  21.7 5.3 %copy-start = (f32[2048]{0:T(1024)S(1)}, f32[2048]{0:T(1024)}, u32[]{:S(2)}) copy-start(f32[2048]{0:T(1024)} %param.19) | copy-start | bytes 24580
  21.7 6.3 %copy-start.1 = (s32[128,2]{0,1:T(2,128)S(1)}, s32[128,2]{0,1:T(2,128)}, u32[]{:S(2)}) copy-start(s32[128,2]{0,1:T(2,128)} %param.21) | copy-start | bytes 3076
  21.7 7.8 %copy-start.2 = (f32[128,2]{0,1:T(2,128)S(1)}, f32[128,2]{0,1:T(2,128)}, u32[]{:S(2)}) copy-start(f32[128,2]{0,1:T(2,128)} %param.22) | copy-start | bytes 3076

commit v2 on v1

--- a/solution.py
+++ b/solution.py
@@ -53,8 +53,7 @@
     rows, width = first.shape
     slots = g.peers * cap
     part = width // parts
-    above = g.device((plane + 1) % g.planes, peer)
-    below = g.device((plane + last) % g.planes, peer)
+    at_end = (plane == 0) | (plane == last)
     loads = [
         pltpu.make_async_copy(src.at[0], dst, w_sem.at[n])
         for n, (src, dst) in enumerate(((w_gate, v_gate), (w_up, v_up), (w_down, v_down)))
@@ -66,19 +65,22 @@
     g.greet(plane, peer)
 
     def cols(c):
-        return pl.ds(c * part, part)
+        return pl.ds(c * part if isinstance(c, int) else pl.multiple_of(c * part, part), part)
+
+    def toward(way):
+        return g.device((plane + (last if way else 1)) % g.planes, peer)
 
     def mine(at):
         return pl.ds(pl.multiple_of(at * cap, cap), cap)
 
     def table_copy(b, way, own):
         src = table if own else tables.at[b]
-        return remote(src, tables.at[b], tab_send.at[way, b], tab_recv.at[b], above if way == 0 else below)
+        return remote(src, tables.at[b], tab_send.at[way, b], tab_recv.at[b], toward(way))
 
     def block_copy(b, way, c, own):
         src = first.at[:, cols(c)] if own else held.at[b, :, cols(c)]
         return remote(
-            src, held.at[b, :, cols(c)], blk_send.at[way, b, c], blk_recv.at[b, c], above if way == 0 else below
+            src, held.at[b, :, cols(c)], blk_send.at[way, b, c], blk_recv.at[b, c], toward(way)
         )
 
     def has_way(way):
@@ -151,16 +153,17 @@
             came.at[way, b, :, cols(c)],
             sum_send.at[b, c],
             sum_recv.at[way, b, c],
-            above if way == 0 else below,
-        )
-
-    def chains(k):
-        yield 0, k, k > plane, plane > 0
-        yield 1, last - k, last - k < plane, plane < last
+            toward(way),
+        )
 
     cut = 256
 
-    def expert(b):
+    def answers(b, c):
+        for d in range(1, g.peers):
+            ans_copy(b, d, c).start()
+        ans_own_copy(b, c).start()
+
+    def expert(b, reply=True):
         for c in range(parts):
             own_copy(b, c).wait()
             for d in range(1, g.peers):
@@ -178,50 +181,42 @@
         for c in range(parts):
             answer = jnp.dot(hidden[...], v_down[:, cols(c)], preferred_element_type=jnp.float32)
             out[b, :, cols(c)] = answer.astype(jnp.bfloat16)
-            for d in range(1, g.peers):
-                ans_copy(b, d, c).start()
-            ans_own_copy(b, c).start()
-
-    def experts_near(s):
-        for way, b, valid in near(s):
-            pl.when(valid)(functools.partial(expert, b))
-
-    def combine(k, c):
-        for way, b, valid, relayed in chains(k):
-
-            @pl.when(valid & relayed)
-            def _():
-                total = partial(b, c)
-                sum_copy(b, way, c).wait_recv()
-                sums[b, :, cols(c)] = (total + came[way, b, :, cols(c)].astype(jnp.float32)).astype(jnp.bfloat16)
-                sum_copy(b, way, c).start()
-
-            @pl.when(valid & jnp.logical_not(relayed))
-            def _():
-                sums[b, :, cols(c)] = partial(b, c).astype(jnp.bfloat16)
-                sum_copy(b, way, c).start()
-
-    def arrive(s, c):
-        for way, b, valid in near(s):
-
-            @pl.when(valid)
-            def _():
-                if c == 0:
-                    table_copy(b, way, False).wait_recv()
-
-                    @pl.when(has_way(way))
-                    def _():
-                        table_copy(b, way, False).start()
-
-                block_copy(b, way, c, False).wait_recv()
-
-                @pl.when(has_way(way))
-                def _():
-                    block_copy(b, way, c, False).start()
-
-                place(b, c)
-                if c == 0:
-                    weigh(b)
+            if reply:
+                answers(b, c)
+
+    def reply_late(b):
+        for c in range(parts):
+            answers(b, c)
+
+    def combine(way, b, c, relayed):
+        total = partial(b, c)
+        if relayed:
+            sum_copy(b, way, c).wait_recv()
+            total = total + came[way, b, :, cols(c)].astype(jnp.float32)
+        sums[b, :, cols(c)] = total.astype(jnp.bfloat16)
+        sum_copy(b, way, c).start()
+
+    def arrive(b, c):
+        if c == 0:
+            table_copy(b, 0, False).wait_recv()
+        block_copy(b, 0, c, False).wait_recv()
+        place(b, c)
+        if c == 0:
+            weigh(b)
+
+    def pass_on(b, way, c):
+        if c == 0:
+            table_copy(b, way, False).wait_recv()
+            table_copy(b, way, False).start()
+        block_copy(b, way, c, False).wait_recv()
+        block_copy(b, way, c, False).start()
+        place(b, c)
+        if c == 0:
+            weigh(b)
+
+    def keep():
+        for c in range(parts):
+            h2[:, cols(c)] = residual_scale * first[:, cols(c)].astype(jnp.float32) + partial(plane, c)
 
     for way in range(2):
 
@@ -234,27 +229,78 @@
     for c in range(parts):
         place(plane, c)
     weigh(plane)
-    for s in range(1, g.planes + 1):
+
+    @pl.when(at_end)
+    def _():
+        low = plane == 0
+
+        def other(s):
+            return jnp.where(low, s, last - s)
+
+        def send_back(s, c):
+            for way in range(2):
+                pl.when(low if way == 0 else jnp.logical_not(low))(lambda: combine(way, other(s), c, False))
+
         for c in range(parts):
-            if s < g.planes:
-                arrive(s, c)
-            if s == 1 and c == parts - 2:
-                for load in loads:
-                    load.wait()
-                expert(plane)
-            if s > 1 and c == 0:
-                experts_near(s - 1)
-            if s == 2 and c == parts - 2:
-                for n in range(parts):
-                    h2[:, cols(n)] = residual_scale * first[:, cols(n)].astype(jnp.float32) + partial(plane, n)
+            arrive(other(1), c)
+        for load in loads:
+            load.wait()
+        expert(plane, False)
+        for s in range(2, g.planes + 1):
+            early = min(s - 1, 2) if s < g.planes else parts
+            for c in range(early):
+                if s < g.planes:
+                    arrive(other(s), c)
+            expert(other(s - 1))
             if s == g.planes:
-                combine(s - 1, c)
-            elif s > 1 and c == parts - 2:
-                for n in range(parts // 2):
-                    combine(s - 1, n)
-            elif s > 1 and c == parts - 1:
-                for n in range(parts // 2, parts):
-                    combine(s - 1, n)
+                reply_late(plane)
+            for c in range(early, parts):
+                arrive(other(s), c)
+                if s == 2:
+                    send_back(s - 1, c - early)
+            for c in range(parts - early if s == 2 else 0, parts):
+                send_back(s - 1, c)
+        keep()
+
+    @pl.when(jnp.logical_not(at_end))
+    def _():
+        low = plane == 1
+        far = jnp.where(low, last, 0)
+        close = jnp.where(low, 2, 1)
+        end = jnp.where(low, 0, last)
+
+        def pass_far(c):
+            for way in range(2):
+                pl.when(low if way == 1 else jnp.logical_not(low))(lambda: pass_on(far, way, c))
+
+        def sums_for(b, up, c):
+            for way in range(2):
+                pl.when(up if way == 0 else jnp.logical_not(up))(lambda: combine(way, b, c, True))
+
+        for c in range(parts):
+            pass_on(plane - 1, 0, c)
+            pass_on(plane + 1, 1, c)
+        for load in loads:
+            load.wait()
+        expert(plane, False)
+        pass_far(0)
+        expert(close)
+        pass_far(1)
+        pass_far(2)
+        expert(end, False)
+        pass_far(3)
+        expert(far)
+        reply_late(end)
+        reply_late(plane)
+        for c in range(parts):
+            sums_for(close, low, c)
+        for c in range(parts + 1):
+            if c < parts:
+                sums_for(far, low, c)
+            if c == parts - 1:
+                keep()
+            if c > 0:
+                sums_for(end, jnp.logical_not(low), c - 1)
 
     for c in range(parts):
         for way in range(2):
@@ -266,9 +312,8 @@
 
     final[...] = token_norm(h2[...], gain[...]).astype(jnp.bfloat16)
     for c in range(parts):
-        for k in range(1, g.planes):
-            for way, b, valid, relayed in chains(k):
-                pl.when(valid)(lambda: sum_copy(b, way, c).wait_send())
+        for b in range(g.planes):
+            pl.when(plane != b)(lambda: sum_copy(b, 0, c).wait_send())
         for b in range(g.planes):
             for d in range(1, g.peers):
                 ans_copy(b, d, c).wait_send()

time: 144 us -> 116 us (0.81)
  Pallas kernels: 133 us -> 105 us
    pallas_call x1, Pallas kernels: 111 us -> 83.2 us  [experts(): pl.pallas_call(functools.partial(experts_kernel, g, cap, parts), name='ex...]
where the time goes in v2:
time: 116 us; the launch traced here: 115 us
  Pallas kernels  105 us (91%)
  matrix products  4.97 us (4%)
  local copies, waits for them, and re-layouts  2.76 us (2%)
  other arithmetic  2.72 us (2%)
    pallas_call x1, Pallas kernels, experts(): pl.pallas_call(functools.partial(experts_kernel, g, cap, parts), name='ex...  83.2 us
    pallas_call x1, Pallas kernels, front(): pl.pallas_call(functools.partial(front_kernel, sp, tp), name='front', out...  21.7 us
    dot_general x1, matrix products, per_device(): mix = jnp.dot(owned, point_weight, preferred_element_type=jnp.float32)  4.97 us

profile of v2, /device:TPU:0, one launch (start us, length us, event | category | flops | bytes accessed | tf_op | source)
XLA Modules:
  0.0 115.5 jit_solution(1076079299258312067)
XLA Ops:
  0.0 21.7 %front.1 = bf16[128,2048]{1,0:T(8,128)(2,1)} custom-call(bf16[512,512]{1,0:T(8,128)(2,1)} %value.1, bf16[512,512]{1,0:T(8,128)(2,1)} %gate.1, f32[31,512]{1,0:T(8,128)} %taps.1, f32[1,512]{1,0:T(1,128)} %bitcast.26), custom_call_target="tpu_custom_call" | custom-call | tf_op jit(solution)/shard_map/front/pallas_call | solution.py:526
  21.7 0.0 copy-start
  21.7 0.0 copy-start.1
  21.7 0.0 copy-start.2
  21.7 5.0 %fusion.4 = (f32[128]{0:T(128)S(1)}, f32[128,2048]{1,0:T(8,128)S(1)}) fusion(bf16[128,2048]{1,0:T(8,128)(2,1)} %front.1, bf16[2048,2048]{1,0:T(8,128)(2,1)} %param.17, bf16[128,2048]{1,0:T(8,128)(2,1)} %param.18), kind=kOutput, calls=%fused_computation.17 | convolution fusion | flops 1074790272 | bytes 10486272 | tf_op jit(solution)/shard_map/dot_general | solution.py:581
  26.7 0.3 multiply_reduce_fusion
  27.0 0.0 copy-done
  27.0 1.0 multiply_convert_fusion.first
  28.0 0.0 copy-done.1
  28.0 0.1 copy.14
  28.1 0.1 eq.29
  28.3 0.6 reduce-window.6
  28.9 0.2 slice_reduce_fusion
  29.1 0.1 eq.25
  29.2 0.1 fusion.2
  29.3 0.1 reduce_sum.41
  29.5 0.1 copy.17
  29.6 0.0 copy-done.2
  29.6 0.1 pad.2.clone
  29.7 0.7 maximum_bitcast_fusion.table
  30.4 83.2 %experts.1 = bf16[128,2048]{1,0:T(8,128)(2,1)} custom-call(bf16[128,2048]{1,0:T(8,128)(2,1)} %multiply_convert_fusion.first, f32[8,128]{1,0:T(8,128)} %maximum_bitcast_fusion.table, f32[1,2048]{1,0:T(1,128)} %bitcast.25, bf16[1,2048,1024]{2,1,0:T(8,128)(2,1)} %w_gate.1, bf16[1,2048,1024]{2,1,0:T(8,128)(2,1)} %w_up.1, bf16[1,1024,2048]{2,1,0:T(8,128)(2,1)} %w_down.1), custom_call_target="tpu_custom_call" | custom-call | tf_op jit(solution)/shard_map/experts/pallas_call | solution.py:342
  113.6 1.9 %copy.21 = bf16[128,2048]{1,0:T(8,128)(2,1)} copy(bf16[128,2048]{1,0:T(8,128)(2,1)} %experts.1) | data formatting | bytes 1048576
  (9 shorter events, 0.1 us)
Async XLA Ops:
  21.7 5.3 %copy-start = (f32[2048]{0:T(1024)S(1)}, f32[2048]{0:T(1024)}, u32[]{:S(2)}) copy-start(f32[2048]{0:T(1024)} %param.19) | copy-start | bytes 24580
  21.7 6.3 %copy-start.1 = (s32[128,2]{0,1:T(2,128)S(1)}, s32[128,2]{0,1:T(2,128)}, u32[]{:S(2)}) copy-start(s32[128,2]{0,1:T(2,128)} %param.21) | copy-start | bytes 3076
  21.7 7.8 %copy-start.2 = (f32[128,2]{0,1:T(2,128)S(1)}, f32[128,2]{0,1:T(2,128)}, u32[]{:S(2)}) copy-start(f32[128,2]{0,1:T(2,128)} %param.22) | copy-start | bytes 3076
